TPU v7x, 32 devices: a whole 2x2x4 slice. The times are simulated.
32 devices in a mesh: sp: 8 (over z, y), tp: 4 (over x, core).
Axes of the slice: x: 2, y: 2, z: 4, core: 2. Of those that a mesh axis runs over, the one named last changes fastest.
Arguments:
- latent: bfloat16 [2048, 2048], P('sp'), may hold values from -6 to 6
- context: bfloat16 [1024, 2048], P('sp'), may hold values from -6 to 6
- condition: bfloat16 [2048], replicated, may hold values from -6 to 6
- context_condition: bfloat16 [2048], replicated, may hold values from -6 to 6
- gain_pre: float32 [2048], replicated, may hold values from 0.1 to 1.9
- gain_post: float32 [2048], replicated, may hold values from 0.1 to 1.9
- w_shift: bfloat16 [2048, 2048], P('sp', 'tp'), may hold values from -0.125 to 0.125
- w_scale: bfloat16 [2048, 2048], P('sp', 'tp'), may hold values from -0.125 to 0.125
- w_gate: bfloat16 [2048, 2048], P('sp', 'tp'), may hold values from -0.125 to 0.125
- w_query: bfloat16 [2048, 2048], P(None, 'tp'), may hold values from -0.13258252 to 0.13258252
- w_key: bfloat16 [2048, 2048], P(None, 'tp'), may hold values from -6.629126 to 6.629126
- w_value: bfloat16 [2048, 2048], P(None, 'tp'), may hold values from -0.125 to 0.125
- w_silu: bfloat16 [2048, 2048], P(None, 'tp'), may hold values from -0.125 to 0.125
- offset_bias: float32 [32, 15, 31], P('tp'), may hold values from 1.5 to 3.5
- w_out: bfloat16 [2048, 2048], P('tp'), may hold values from -0.125 to 0.125
Outputs:
- updated: bfloat16 [2048, 2048], P(('sp', 'tp'))
All inputs are finite; a program needn't handle non-finite values.
Results may differ from a plain program's by a relative error of at most 0.01.
Values may be sent and summed in bfloat16 or wider, within the bound.
A program may use at most 64 MiB of HBM per device.

v0:
```python
import jax
import jax.numpy as jnp
import numpy as np
from jax import lax
from jax.sharding import PartitionSpec as P

GRID_W = 64
WIN_ROWS = 8
WIN_COLS = 16


EPSILON = 1e-06


def extended_2(cells, sides, width):
    for axis, dim in sides:
        count = lax.axis_size(axis)
        ends = count - 1
        head = lax.slice_in_dim(cells, 0, width, axis=dim)
        tail = lax.slice_in_dim(cells, cells.shape[dim] - width, cells.shape[dim], axis=dim)
        cells = jnp.concatenate(
            [
                lax.ppermute(tail, axis, [(i, (i + 1) % count) for i in range(ends)]),
                cells,
                lax.ppermute(head, axis, [((i + 1) % count, i) for i in range(ends)]),
            ],
            axis=dim,
        )
    return cells


def normalize(row_block, gain_row):
    values = row_block.astype(jnp.float32)
    return (
        values * lax.rsqrt(jnp.mean(values * values, axis=-1, keepdims=True) + EPSILON) * gain_row
    )


def modulate(row_block, gain_row, shift_row, scale_row):
    return (normalize(row_block, gain_row) * (1.0 + scale_row) + shift_row).astype(jnp.bfloat16)


def product(left, right):
    return jnp.dot(left, right, preferred_element_type=jnp.float32)


def shards(
    latent,
    context,
    condition,
    context_condition,
    gain_pre,
    gain_post,
    w_shift,
    w_scale,
    w_gate,
    w_query,
    w_key,
    w_value,
    w_silu,
    offset_bias,
    w_out,
):
    sp_index = lax.axis_index("sp")
    tp_index = lax.axis_index("tp")
    in_rows, local_cols = w_shift.shape
    tokens, model_width = latent.shape
    active = jax.nn.silu(jnp.stack([condition, context_condition]).astype(jnp.float32)).astype(
        jnp.bfloat16
    )
    own_active = lax.dynamic_slice_in_dim(active, sp_index * in_rows, in_rows, 1)
    stacked = jnp.stack([w_shift, w_scale, w_gate])
    partial_value = jnp.einsum(
        "ai,mij->maj", own_active, stacked, preferred_element_type=jnp.float32
    )
    summed = lax.psum(partial_value, "sp")
    modulation = lax.all_gather(summed, "tp", axis=2, tiled=True)
    shifts, scales, gating = (modulation[0], modulation[1], modulation[2])
    normed = modulate(context, gain_pre, shifts[1], scales[1])
    context_kv = lax.all_gather(
        jnp.concatenate([product(normed, w_key), product(normed, w_value)], axis=1).astype(
            jnp.bfloat16
        ),
        "sp",
        axis=0,
        tiled=True,
    )
    hidden = modulate(latent, gain_pre, shifts[0], scales[0])
    queries = product(hidden, w_query).astype(jnp.bfloat16)
    keys_latent = product(hidden, w_key).astype(jnp.bfloat16)
    values_latent = product(hidden, w_value).astype(jnp.bfloat16)
    silu_gate = product(hidden, w_silu).astype(jnp.bfloat16)
    head_count = offset_bias.shape[0]
    head_width = local_cols // head_count
    grid_rows = tokens // GRID_W
    kv_grid = jnp.concatenate([keys_latent, values_latent], axis=1).reshape(
        grid_rows, GRID_W, 2 * local_cols
    )
    extended = extended_2(kv_grid, (("sp", 0),), WIN_ROWS // 2)
    blocks = GRID_W // WIN_COLS
    key_span = 2 * WIN_COLS
    block_start = np.clip(np.arange(blocks) * WIN_COLS - WIN_COLS // 2, 0, GRID_W - key_span)
    query_col = np.arange(blocks)[:, None] * WIN_COLS + np.arange(WIN_COLS)[None, :]
    key_col = block_start[:, None] + np.arange(key_span)[None, :]
    window_start = np.clip(query_col - WIN_COLS // 2, 0, GRID_W - WIN_COLS)
    inside_cols = (key_col[:, None, :] >= window_start[:, :, None]) & (
        key_col[:, None, :] < window_start[:, :, None] + WIN_COLS
    )
    inside_window = np.broadcast_to(
        inside_cols[:, :, None, :], (blocks, WIN_COLS, WIN_ROWS, key_span)
    ).reshape(blocks, WIN_COLS, WIN_ROWS * key_span)[None, :, None, :, :]
    col_offset = np.clip(
        key_col[:, None, :] - query_col[:, :, None] + WIN_COLS - 1, 0, 2 * WIN_COLS - 2
    )
    col_table = (col_offset[..., None] == np.arange(2 * WIN_COLS - 1)).astype(np.float32)
    total_rows = grid_rows * lax.axis_size("sp")
    local_rows = jnp.arange(grid_rows, dtype=jnp.int32)
    global_row = sp_index * grid_rows + local_rows
    row_start = jnp.clip(global_row - WIN_ROWS // 2, 0, total_rows - WIN_ROWS)
    band_first = row_start - sp_index * grid_rows + WIN_ROWS // 2
    row_offset = (
        row_start[:, None]
        + jnp.arange(WIN_ROWS, dtype=jnp.int32)[None, :]
        - global_row[:, None]
        + WIN_ROWS
        - 1
    )
    row_table = (row_offset[..., None] == jnp.arange(2 * WIN_ROWS - 1, dtype=jnp.int32)).astype(
        jnp.float32
    )
    position = (
        band_first[:, None, None, None] + jnp.arange(WIN_ROWS, dtype=jnp.int32)[None, None, :, None]
    ) * GRID_W + jnp.asarray(key_col, jnp.int32)[None, :, None, :]
    flat_rows = extended.reshape(-1, 2 * local_cols)
    window_kv = jnp.take(flat_rows, position.reshape(-1), axis=0).reshape(
        grid_rows, blocks, WIN_ROWS * key_span, 2 * local_cols
    )
    window_keys = window_kv[..., :local_cols].reshape(
        grid_rows, blocks, WIN_ROWS * key_span, head_count, head_width
    )
    window_values = window_kv[..., local_cols:].reshape(
        grid_rows, blocks, WIN_ROWS * key_span, head_count, head_width
    )
    context_keys = context_kv[:, :local_cols].reshape(-1, head_count, head_width)
    context_values = context_kv[:, local_cols:].reshape(-1, head_count, head_width)
    query_blocks = queries.reshape(grid_rows, blocks, WIN_COLS, head_count, head_width)
    score_scale = head_width ** (-0.5)
    by_column = jnp.einsum(
        "hae,bqwe->hbqwa", offset_bias, jnp.asarray(col_table), precision=lax.Precision.HIGHEST
    )
    offset_terms = jnp.einsum(
        "rva,hbqwa->rbhqvw", row_table, by_column, precision=lax.Precision.HIGHEST
    ).reshape(grid_rows, blocks, head_count, WIN_COLS, WIN_ROWS * key_span)
    window_scores = (
        jnp.einsum(
            "rbqhd,rbkhd->rbhqk", query_blocks, window_keys, preferred_element_type=jnp.float32
        )
        * score_scale
    )
    window_scores = jnp.where(inside_window, window_scores + offset_terms, -jnp.inf)
    context_scores = (
        jnp.einsum(
            "rbqhd,khd->rbhqk", query_blocks, context_keys, preferred_element_type=jnp.float32
        )
        * score_scale
    )
    maximum = jnp.maximum(jnp.max(window_scores, axis=-1), jnp.max(context_scores, axis=-1))[
        ..., None
    ]
    window_exp = jnp.exp(window_scores - maximum)
    context_exp = jnp.exp(context_scores - maximum)
    denominator = jnp.sum(window_exp, axis=-1, keepdims=True) + jnp.sum(
        context_exp, axis=-1, keepdims=True
    )
    window_weights = (window_exp / denominator).astype(jnp.bfloat16)
    context_weights = (context_exp / denominator).astype(jnp.bfloat16)
    attended = jnp.einsum(
        "rbhqk,rbkhd->rbqhd", window_weights, window_values, preferred_element_type=jnp.float32
    )
    attended = attended + jnp.einsum(
        "rbhqk,khd->rbqhd", context_weights, context_values, preferred_element_type=jnp.float32
    )
    attended = attended.reshape(tokens, local_cols)
    gated_heads = (jax.nn.silu(silu_gate.astype(jnp.float32)) * attended).astype(jnp.bfloat16)
    out_rows = tokens // lax.axis_size("tp")
    branch = lax.psum_scatter(
        product(gated_heads, w_out).astype(jnp.bfloat16), "tp", scatter_dimension=0, tiled=True
    )
    own_rows = lax.dynamic_slice_in_dim(latent, tp_index * out_rows, out_rows, 0)
    updated = own_rows.astype(jnp.float32) + gating[0] * normalize(branch, gain_post)
    return updated.astype(jnp.bfloat16)


def solution(mesh):
    in_specs = (
        P("sp", None),
        P("sp", None),
        P(),
        P(),
        P(),
        P(),
        P("sp", "tp"),
        P("sp", "tp"),
        P("sp", "tp"),
        P(None, "tp"),
        P(None, "tp"),
        P(None, "tp"),
        P(None, "tp"),
        P("tp", None, None),
        P("tp", None),
    )
    out_specs = P(("sp", "tp"), None)
    return jax.shard_map(shards, mesh=mesh, in_specs=in_specs, out_specs=out_specs, check_vma=False)
```

profile of v0, /device:TPU:0, one launch (start us, length us, event | category | flops | bytes accessed | tf_op | source)
XLA Modules:
  0.0 194.9 jit_solution(9264720837811773831)
XLA Ops:
  6.6 1.7 fusion.9
  8.2 0.7 stack.25
  9.6 1.4 convolution_bitcast_fusion.1
  11.0 38.9 %psum.7 = f32[3,2,512]{2,1,0:T(2,128)S(1)} all-reduce(f32[3,2,512]{2,1,0:T(2,128)S(1)} %convolution_bitcast_fusion.1), channel_id=1, replica_groups=mesh['sp'=8,'tp'=4] {'sp'}, use_global_device_ids=true, to_apply=%region_0.1 | all-reduce | flops 3072 | bytes 24576 | tf_op jit(solution)/shard_map/psum | solution.py:76
  49.9 5.2 %all_gather.6 = f32[3,2,2048]{2,1,0:T(2,128)S(1)} all-gather(f32[3,2,512]{2,1,0:T(2,128)S(1)} %psum.7), channel_id=1, replica_groups=mesh['sp'=8,'tp'=4] {'tp'}, dimensions={2}, use_global_device_ids=true | all-gather | bytes 61440 | tf_op jit(solution)/shard_map/all_gather | solution.py:77
  55.1 2.5 %convolution_convert_fusion.3 = bf16[256,512]{1,0:T(8,128)(2,1)S(1)} fusion(bf16[2048,512]{1,0:T(8,128)(2,1)} %param.28, bf16[256,2048]{1,0:T(8,128)(2,1)S(1)} %copy-done.4, f32[2048]{0:T(1024)S(1)} %bitcast.96, f32[2048]{0:T(1024)S(1)} %bitcast.100, f32[2048]{0:T(1024)S(1)} %copy-done.15, f32[256]{0:T(256)S(1)} %add_rsqrt_fusion), kind=kOutput, calls=%fused_computation.33 | convolution fusion | flops 540147712 | bytes 3433472 | tf_op jit(solution)/shard_map/dot_general | solution.py:44
  57.7 0.8 convolution_convert_fusion.2
  58.5 1.4 collective-permute-start.1
  59.9 5.4 %collective-permute-start = (bf16[4,64,1024]{2,1,0:T(8,128)(2,1)S(1)}, bf16[4,64,1024]{2,1,0:T(8,128)(2,1)}, u32[]{:S(2)}, u32[]{:S(2)}) collective-permute-start(bf16[4,64,1024]{2,1,0:T(8,128)(2,1)S(1)} %bitcast.90), channel_id=1, source_target_pairs={{0,4},{4,8},{8,12},{12,16},{16,20},{20,24},{24,28},{1,5},{5,9},{9,... | collective-permute-start | bytes 1572872 | tf_op jit(solution)/shard_map/ppermute | solution.py:23
  66.5 0.7 pad_maximum_fusion.2
  67.7 6.2 %fusion.42 = f32[4,16,32,8,15]{2,4,1,0,3:T(8,128)S(1)} fusion(f32[4,16,32,31,1]{3,2,1,0,4:T(8,128)} %constant.79, f32[8,15,31,1,1]{2,0,1,4,3:T(8,128)S(1)} %bitcast.93), kind=kOutput, calls=%fused_computation.66 | convolution fusion | flops 91422720 | bytes 1251872 | tf_op jit(solution)/shard_map/hae,bqwe->hbqwa/dot_general | solution.py:148
  73.9 5.8 %fusion.6 = f32[4,4,8,16,8,32]{5,4,0,3,1,2:T(8,128)} fusion(f32[4,16,32,8,15]{2,4,1,0,3:T(8,128)S(1)} %fusion.42, s32[4,8]{1,0:T(4,128)S(1)} %subtract_add_fusion), kind=kOutput, calls=%fused_computation.11 | convolution fusion | flops 94372320 | bytes 3080320 | tf_op jit(solution)/shard_map/rva,hbqwa->rbhqvw/dot_general | solution.py:151
  79.7 0.7 convolution_convert_fusion.1
  81.0 7.4 %reshape.240 = f32[4,4,8,16,256]{4,0,3,1,2:T(4,128)} reshape(f32[4,4,8,16,8,32]{5,4,0,3,1,2:T(8,128)} %fusion.6) | data formatting | bytes 4194304 | tf_op jit(solution)/shard_map/reshape | solution.py:153
  88.4 2.6 %pad_maximum_fusion = bf16[12,64,1024]{2,1,0:T(8,128)(2,1)} fusion(bf16[4,64,1024]{2,1,0:T(8,128)(2,1)} %collective-permute-done.1, bf16[4,64,1024]{2,1,0:T(8,128)(2,1)S(1)} %bitcast.91, bf16[4,64,1024]{2,1,0:T(8,128)(2,1)} %collective-permute-done), kind=kLoop, calls=%fused_computation.25 | loop fusion | flops 1572864 | bytes 3145728 | tf_op jit(solution)/shard_map/concatenate | solution.py:21
  91.0 22.5 %gather_fusion = bf16[4096,1024]{1,0:T(8,128)(2,1)} fusion(bf16[768,1024]{1,0:T(8,128)(2,1)} %bitcast.84, s32[4096]{0:T(1024)S(1)} %broadcast_clamp_fusion), kind=kCustom, calls=%fused_computation | custom fusion | bytes 16793600 | tf_op jit(solution)/shard_map/jit(_take)/gather | solution.py:135
  113.6 11.4 %copy.50 = bf16[4,4,256,1024]{2,3,1,0:T(8,128)(2,1)} copy(bf16[4,4,256,1024]{3,2,1,0:T(8,128)(2,1)} %bitcast.85) | data formatting | bytes 16777216 | tf_op jit(solution)/shard_map/jit(_take)/gather | solution.py:135
  124.9 7.4 %broadcast_select_fusion = bf16[4,4,256,1024]{2,3,1,0:T(8,128)(2,1)} fusion(bf16[4,4,256,1024]{2,3,1,0:T(8,128)(2,1)} %copy.50, pred[4,4,256]{2,1,0:T(4,128)(4,1)S(1)} %fusion.46), kind=kLoop, calls=%fused_computation.5 | loop fusion | flops 4194304 | bytes 16781312 | tf_op jit(solution)/shard_map/jit(_take)/select_n | solution.py:135
  132.3 5.2 %fusion.64 = (bf16[4,4,256,512]{2,3,1,0:T(8,128)(2,1)}, bf16[4,4,256,512]{2,3,1,0:T(8,128)(2,1)S(1)}) fusion(bf16[4,4,256,1024]{2,3,1,0:T(8,128)(2,1)} %broadcast_select_fusion), kind=kLoop, calls=%fused_computation.97 | loop fusion | bytes 16777216 | tf_op jit(solution)/shard_map/slice | solution.py:141
  137.6 2.2 %fusion.67 = (f32[4,4,8,16]{3,2,1,0:T(8,128)S(1)}, f32[4,4,8,16,256]{4,3,2,1,0:T(8,128)}) fusion(f32[4,4,8,16,256]{4,0,3,1,2:T(4,128)S(1)} %copy-done.1, bf16[4,4,256,8,64]{2,4,3,1,0:T(8,128)(2,1)S(1)} %bitcast.86, bf16[4,4,16,8,64]{4,3,2,1,0:T(8,128)(2,1)S(1)} %reshape.219, pred[4,16,256]{2,1,0:T(8,128)(4,1)S(1)} %copy-done.8), kind=kOutput, calls=%fused_computation.100 | convolution fusion | flops 69203968 | bytes 8675328 | tf_op jit(solution)/shard_map/rbqhd,rbkhd->rbhqk/dot_general | solution.py:155
  139.8 3.0 %fusion.65 = (bf16[1024,512]{1,0:T(8,128)(2,1)}, bf16[1024,512]{1,0:T(8,128)(2,1)}) fusion(bf16[1024,1024]{1,0:T(8,128)(2,1)} %all-gather.2.cloned.1.call-done), kind=kLoop, calls=%fused_computation.98 | loop fusion | bytes 4194304 | tf_op jit(solution)/shard_map/slice | solution.py:144
  142.8 2.3 %copy.54 = bf16[1024,512]{0,1:T(8,128)(2,1)} copy(bf16[1024,512]{1,0:T(8,128)(2,1)} %get-tuple-element.7) | data formatting | bytes 2097152 | tf_op jit(solution)/shard_map/slice | solution.py:144
  145.1 2.3 %copy.59 = bf16[1024,512]{0,1:T(8,128)(2,1)} copy(bf16[1024,512]{1,0:T(8,128)(2,1)} %get-tuple-element.8) | data formatting | bytes 2097152 | tf_op jit(solution)/shard_map/slice | solution.py:145
  147.4 2.7 %bitcast_reduce_fusion = (f32[4,4,8,16]{3,1,0,2:T(4,128)S(1)}, f32[8,1024,4,4,16]{1,4,3,2,0:T(8,128)S(1)}) fusion(bf16[1024,8,64,1,1]{0,2,4,3,1:T(8,128)(2,1)} %bitcast.87, bf16[4,4,16,8,64]{4,3,2,1,0:T(8,128)(2,1)S(1)} %reshape.219), kind=kOutput, calls=%fused_computation.2 | convolution fusion | flops 272627712 | bytes 9707520 | tf_op jit(solution)/shard_map/rbqhd,khd->rbhqk/dot_general | solution.py:162
  150.9 1.8 fusion.1
  152.8 2.4 %fusion.16 = f32[4,4,16,8,64]{4,2,3,1,0:T(8,128)S(1)} fusion(bf16[1024,8,64,1,1]{0,2,1,4,3:T(8,128)(2,1)S(1)} %bitcast.92, f32[8,1024,4,4,16]{1,4,3,2,0:T(8,128)S(1)} %get-tuple-element.17, f32[4,4,8,16]{3,1,0,2:T(4,128)S(1)} %copy.60, f32[4,4,8,16]{3,1,0,2:T(4,128)S(1)} %copy.57), kind=kOutput, calls=%fused_computation.26 | convolution fusion | flops 276824064 | bytes 9977856 | tf_op jit(solution)/shard_map/rbhqk,khd->rbqhd/dot_general | solution.py:180
  155.2 1.7 fusion.19
  157.3 1.1 reshape.224
  158.4 4.4 %convolution_convert_fusion = bf16[256,2048]{1,0:T(8,128)(2,1)} fusion(bf16[512,2048]{1,0:T(8,128)(2,1)S(1)} %copy-done, f32[256,512]{1,0:T(8,128)} %reshape.224, bf16[2048,512]{1,0:T(8,128)(2,1)} %param.30, bf16[256,2048]{1,0:T(8,128)(2,1)} %param.18, f32[2048]{0:T(1024)S(1)} %bitcast.99, f32[2048]{0:T(1024)S(1)} %bitcast.103, f32[2048]{0:T(1024)S(1)} %copy-done.15, ...), kind=kOutput, calls=%fused_computation.14 | convolution fusion | flops 1078460416 | bytes 6841344 | tf_op jit(solution)/shard_map/dot_general | solution.py:44
  162.8 22.2 %reduce-scatter.2.cloned.1.call-done = bf16[64,2048]{1,0:T(8,128)(2,1)} async-done(((bf16[256,2048]{1,0:T(8,128)(2,1)}), bf16[64,2048]{1,0:T(8,128)(2,1)}) %reduce-scatter.2.cloned.1.call-update) | async-done | bytes 262160 | tf_op jit(solution)/shard_map/reduce_scatter | solution.py:186
  185.0 1.1 fusion.33
  186.1 1.9 fusion.37
  (69 shorter events, 4.2 us)
Async XLA Ops:
  6.5 151.8 %copy-start = (bf16[512,2048]{1,0:T(8,128)(2,1)S(1)}, bf16[512,2048]{1,0:T(8,128)(2,1)}, u32[]{:S(2)}) copy-start(bf16[512,2048]{1,0:T(8,128)(2,1)} %param.32) | copy-start | bytes 6291460
  6.5 48.6 %copy-start.4 = (bf16[256,2048]{1,0:T(8,128)(2,1)S(1)}, bf16[256,2048]{1,0:T(8,128)(2,1)}, u32[]{:S(2)}) copy-start(bf16[256,2048]{1,0:T(8,128)(2,1)} %param.18) | copy-start | bytes 3145732
  6.5 48.6 %copy-start.15 = (f32[2048]{0:T(1024)S(1)}, f32[2048]{0:T(1024)}, u32[]{:S(2)}) copy-start(f32[2048]{0:T(1024)} %param.22) | copy-start | bytes 24580
  6.5 133.2 %all-gather.2.cloned.1.call-start = ((), (), s32[]{:S(2)}) async-start(), calls=%async_computation.1 | async-start | bytes 2359296 | tf_op jit(solution)/shard_map/all_gather | solution.py:80
  55.1 2.5 %copy-start.12 = (bf16[2048,512]{1,0:T(8,128)(2,1)S(1)}, bf16[2048,512]{1,0:T(8,128)(2,1)}, u32[]{:S(2)}) copy-start(bf16[2048,512]{1,0:T(8,128)(2,1)} %param.29) | copy-start | bytes 6291460
  57.6 7.6 %copy-start.7 = (bf16[128,2048]{1,0:T(8,128)(2,1)S(1)}, bf16[128,2048]{1,0:T(8,128)(2,1)}, u32[]{:S(2)}) copy-start(bf16[128,2048]{1,0:T(8,128)(2,1)} %param.19) | copy-start | bytes 1572868
  58.5 7.5 %copy-start.13 = (bf16[2048,512]{1,0:T(8,128)(2,1)S(1)}, bf16[2048,512]{1,0:T(8,128)(2,1)}, u32[]{:S(2)}) copy-start(bf16[2048,512]{1,0:T(8,128)(2,1)} %param.28) | copy-start | bytes 6291460
  58.5 29.9 %collective-permute-start.1 = (bf16[4,64,1024]{2,1,0:T(8,128)(2,1)S(1)}, bf16[4,64,1024]{2,1,0:T(8,128)(2,1)}, u32[]{:S(2)}, u32[]{:S(2)}) collective-permute-start(bf16[4,64,1024]{2,1,0:T(8,128)(2,1)S(1)} %bitcast.89), channel_id=1, source_target_pairs={{4,0},{8,4},{12,8},{16,12},{20,16},{24,20},{28,24},{5,1},{9,5},{13... | collective-permute-start | bytes 1572872 | tf_op jit(solution)/shard_map/ppermute | solution.py:25
  59.9 28.5 %collective-permute-start = (bf16[4,64,1024]{2,1,0:T(8,128)(2,1)S(1)}, bf16[4,64,1024]{2,1,0:T(8,128)(2,1)}, u32[]{:S(2)}, u32[]{:S(2)}) collective-permute-start(bf16[4,64,1024]{2,1,0:T(8,128)(2,1)S(1)} %bitcast.90), channel_id=1, source_target_pairs={{0,4},{4,8},{8,12},{12,16},{16,20},{20,24},{24,28},{1,5},{5,9},{9,... | collective-permute-start | bytes 1572872 | tf_op jit(solution)/shard_map/ppermute | solution.py:23
  66.0 1.4 copy-start.11
  66.0 1.6 copy-start.9
  67.3 117.7 %reduce-scatter.2.cloned.1.call-start = ((), (), s32[]{:S(2)}) async-start(), calls=%async_computation.2 | async-start | bytes 1310720 | tf_op jit(solution)/shard_map/reduce_scatter | solution.py:186
  73.9 5.8 %copy-start.5 = (bf16[256,2048]{1,0:T(8,128)(2,1)S(1)}, bf16[256,2048]{1,0:T(8,128)(2,1)}, u32[]{:S(2)}) copy-start(bf16[256,2048]{1,0:T(8,128)(2,1)} %param.18) | copy-start | bytes 3145732
  73.9 5.8 %copy-start.14 = (bf16[2048,512]{1,0:T(8,128)(2,1)S(1)}, bf16[2048,512]{1,0:T(8,128)(2,1)}, u32[]{:S(2)}) copy-start(bf16[2048,512]{1,0:T(8,128)(2,1)} %param.27) | copy-start | bytes 6291460
  132.3 5.2 %copy-start.1 = (f32[4,4,8,16,256]{4,0,3,1,2:T(4,128)S(1)}, f32[4,4,8,16,256]{4,0,3,1,2:T(4,128)}, u32[]{:S(2)}) copy-start(f32[4,4,8,16,256]{4,0,3,1,2:T(4,128)} %reshape.240) | copy-start | bytes 6291460
  132.3 5.2 %copy-start.8 = (pred[4,16,256]{2,1,0:T(8,128)(4,1)S(1)}, pred[4,16,256]{2,1,0:T(8,128)(4,1)}, u32[]{:S(2)}) copy-start(pred[4,16,256]{2,1,0:T(8,128)(4,1)} %constant.78) | copy-start | bytes 49156
  147.4 2.8 %copy-start.2 = (f32[4,4,8,16,256]{4,3,2,1,0:T(8,128)S(1)}, f32[4,4,8,16,256]{4,3,2,1,0:T(8,128)}, u32[]{:S(2)}) copy-start(f32[4,4,8,16,256]{4,3,2,1,0:T(8,128)} %get-tuple-element.15) | copy-start | bytes 6291460
  150.9 1.9 copy-start.6
  152.8 2.4 %copy-start.3 = (bf16[4,4,256,512]{2,3,1,0:T(8,128)(2,1)S(1)}, bf16[4,4,256,512]{2,3,1,0:T(8,128)(2,1)}, u32[]{:S(2)}) copy-start(bf16[4,4,256,512]{2,3,1,0:T(8,128)(2,1)} %get-tuple-element.5) | copy-start | bytes 12582916
  158.4 27.8 %copy-start.10 = (f32[2048]{0:T(1024)S(1)}, f32[2048]{0:T(1024)}, u32[]{:S(2)}) copy-start(f32[2048]{0:T(1024)} %param.23) | copy-start | bytes 24580
Sparse Core Ops, SparseCore 0:
  67.4 48.7 all-gather.1
  162.9 22.0 reduce-scatter.1
where the time goes:
time: 196 us; the launch traced here: 195 us
  local copies, waits for them, and re-layouts  57.6 us (29%)
  blocking collectives  44.1 us (22%)
  matrix products  31.8 us (16%)
  waiting for transfers between devices  22.2 us (11%)
  other arithmetic  18.6 us (9%)
  between operations  13.8 us (7%)
  starting transfers between devices  6.83 us (3%)
    psum x1, blocking collectives, shards(): summed = lax.psum(partial_value, 'sp')  38.9 us
    gather x2, local copies, waits for them, and re-layouts, shards(): jnp.take(flat_rows, position.reshape(-1), axis=0)  33.9 us
    reduce_scatter x1, waiting for transfers between devices, shards(): lax.psum_scatter(product(gated_heads, w_out).astype(jnp.bfloat16), 'tp',...  22.2 us
    dot_general x6, matrix products, product(): return jnp.dot(left, right, preferred_element_type=jnp.float32)  9.43 us
    select_n x2, other arithmetic, shards(): jnp.take(flat_rows, position.reshape(-1), axis=0)  7.45 us
    reshape x1, local copies, waits for them, and re-layouts, shards(): offset_terms = jnp.einsum('rva,hbqwa->rbhqvw', row_table, by_column, prec...  7.36 us
    dot_general x1, matrix products, shards(): jnp.einsum('hae,bqwe->hbqwa', offset_bias, jnp.asarray(col_table), precis...  6.16 us
    dot_general x1, matrix products, shards(): jnp.einsum('rva,hbqwa->rbhqvw', row_table, by_column, precision=lax.Preci...  5.84 us
  transfers between devices with their start and end apart: 4, of which 1 were waited for; matrix products, arithmetic and copies ran while one was open for 38% of the time, Pallas kernels for 0%

commit v1 on v0

v1 whole, which is shorter than its diff:
```python
import functools

import jax
import jax.numpy as jnp
from jax import lax
from jax.experimental import pallas as pl
from jax.experimental.pallas import tpu as pltpu
from jax.sharding import PartitionSpec as P

GRID_W = 64
WIN_ROWS = 8
WIN_COLS = 16
EPSILON = 1e-06
MASKED = -1e30
F32 = jnp.float32
BF16 = jnp.bfloat16
TILE = 256


def remote(src, dst, send, recv, where):
    return pltpu.make_async_remote_copy(
        src_ref=src,
        dst_ref=dst,
        send_sem=send,
        recv_sem=recv,
        device_id=where,
        device_id_type=pl.DeviceIdType.MESH,
    )


def dot(a, b):
    return jnp.dot(a, b, preferred_element_type=F32)


def dot_t(a, b):
    return lax.dot_general(a, b, (((1,), (1,)), ((), ())), preferred_element_type=F32)


def kernel(
    S,
    T,
    active,
    gain_pre,
    gain_post,
    table_rows,
    latent_hbm,
    context_hbm,
    wsh_hbm,
    wsc_hbm,
    wga_hbm,
    wq_hbm,
    wk_hbm,
    wv_hbm,
    ws_hbm,
    wo_hbm,
    out,
    lat,
    ctx,
    wmod,
    wall,
    wo,
    part,
    modbuf,
    modfull,
    modrow,
    norm_lat,
    norm_ctx,
    hid_lat,
    hid_ctx,
    qg,
    kv,
    ckv,
    table,
    gated,
    prod,
    terms,
    load_sem,
    a_send,
    a_recv,
    b_send,
    b_recv,
    y_send,
    y_recv,
    z_send,
    z_recv,
    h_send,
    h_recv,
    r_send,
    r_recv,
):
    s = lax.axis_index("sp")
    t = lax.axis_index("tp")
    tokens, width = lat.shape
    n_ctx = ctx.shape[0]
    cols = wo.shape[0]
    heads = table.shape[0]
    rows = tokens // GRID_W
    Y = max(1, T // 2)
    if S % Y:
        Y = 1
    Z = S // Y
    z = s // Y
    y = s % Y

    loads = []
    for i, (src, dst) in enumerate(
        [
            (wsh_hbm, wmod.at[0]),
            (wsc_hbm, wmod.at[1]),
            (wga_hbm, wmod.at[2]),
            (context_hbm, ctx),
            (latent_hbm, lat),
            (wk_hbm, wall.at[:, pl.ds(0, cols)]),
            (wv_hbm, wall.at[:, pl.ds(cols, cols)]),
            (wq_hbm, wall.at[:, pl.ds(2 * cols, cols)]),
            (ws_hbm, wall.at[:, pl.ds(3 * cols, cols)]),
            (wo_hbm, wo),
        ]
    ):
        copy = pltpu.make_async_copy(src, dst, load_sem.at[i])
        copy.start()
        loads.append(copy)

    barrier = pltpu.get_barrier_semaphore()
    for d in range(1, S):
        pl.semaphore_signal(
            barrier, inc=1, device_id={"sp": lax.rem(s + d, S)}, device_id_type=pl.DeviceIdType.MESH
        )
    for d in range(1, T):
        pl.semaphore_signal(
            barrier, inc=1, device_id={"tp": lax.rem(t + d, T)}, device_id_type=pl.DeviceIdType.MESH
        )

    part[...] = jnp.zeros_like(part)
    for i in range(3):
        loads[i].wait()
        part[2 * i : 2 * i + 2, :] = dot(active[...], wmod[i])[0:2]
    pl.semaphore_wait(barrier, S - 1 + T - 1)

    a_copies = []
    for d in range(1, S):
        copy = remote(
            part, modbuf.at[s], a_send.at[d - 1], a_recv.at[d - 1], {"sp": lax.rem(s + d, S)}
        )
        copy.start()
        a_copies.append(copy)

    def normalise(src, dst):
        step = 32

        @pl.loop(0, src.shape[0] // step)
        def _(i):
            at = pl.ds(pl.multiple_of(i * step, step), step)
            v = src[at, :].astype(F32)
            inv = lax.rsqrt(jnp.mean(v * v, axis=-1, keepdims=True) + EPSILON)
            dst[at, :] = v * inv * gain_pre[...]

    loads[3].wait()
    normalise(ctx, norm_ctx)
    loads[4].wait()

    modbuf[s] = part[...]
    for copy in a_copies:
        copy.wait()
    modfull[t] = jnp.sum(modbuf[...], axis=0)
    b_copies = []
    for d in range(1, T):
        copy = remote(
            modfull.at[t],
            modfull.at[t],
            b_send.at[d - 1],
            b_recv.at[d - 1],
            {"tp": lax.rem(t + d, T)},
        )
        copy.start()
        b_copies.append(copy)

    normalise(lat, norm_lat)

    for copy in b_copies:
        copy.wait()
    for j in range(T):
        modrow[:, j * cols : (j + 1) * cols] = modfull[j]

    def modulate(src, dst, shift, scale):
        step = 32

        @pl.loop(0, src.shape[0] // step)
        def _(i):
            at = pl.ds(pl.multiple_of(i * step, step), step)
            v = src[at, :] * (1.0 + modrow[scale : scale + 1, :]) + modrow[shift : shift + 1, :]
            dst[at, :] = v.astype(BF16)

    modulate(norm_ctx, hid_ctx, 1, 3)
    loads[5].wait()
    loads[6].wait()
    own_ctx = pl.ds(pl.multiple_of(s * n_ctx, n_ctx), n_ctx)

    @pl.loop(0, 2 * cols // TILE)
    def _(i):
        at = pl.ds(pl.multiple_of(i * TILE, TILE), TILE)
        ckv[own_ctx, at] = dot(hid_ctx[...], wall[:, at]).astype(BF16)

    y_copies = []
    for d in range(1, Y):
        copy = remote(
            ckv.at[own_ctx],
            ckv.at[own_ctx],
            y_send.at[d - 1],
            y_recv.at[d - 1],
            {"sp": z * Y + lax.rem(y + d, Y)},
        )
        copy.start()
        y_copies.append(copy)

    modulate(norm_lat, hid_lat, 0, 2)

    @pl.loop(0, 2 * cols // TILE)
    def _(i):
        at = pl.ds(pl.multiple_of(i * TILE, TILE), TILE)
        kv[tokens : 2 * tokens, at] = dot(hid_lat[...], wall[:, at]).astype(BF16)

    own_kv = kv.at[pl.ds(tokens, tokens)]
    to_next = remote(
        own_kv, kv.at[pl.ds(0, tokens)], h_send.at[0], h_recv.at[0], {"sp": lax.rem(s + 1, S)}
    )
    to_prev = remote(
        own_kv,
        kv.at[pl.ds(2 * tokens, tokens)],
        h_send.at[1],
        h_recv.at[1],
        {"sp": lax.rem(s + S - 1, S)},
    )

    for copy in y_copies:
        copy.wait()

    def block_of(k):
        size = Y * n_ctx
        return ckv.at[pl.ds(pl.multiple_of(k * size, size), size)]

    def up(k):
        return remote(
            block_of(z - k),
            block_of(z - k),
            z_send.at[0, k],
            z_recv.at[0, k],
            {"sp": lax.rem(s + Y, S)},
        )

    def down(k):
        return remote(
            block_of(z + k),
            block_of(z + k),
            z_send.at[1, k],
            z_recv.at[1, k],
            {"sp": lax.rem(s + S - Y, S)},
        )

    def send_up(k):
        return (z - k >= 0) & (z < Z - 1)

    def send_down(k):
        return (z + k <= Z - 1) & (z > 0)

    def z_start(k):
        @pl.when(send_up(k))
        def _():
            up(k).start()

        @pl.when(send_down(k))
        def _():
            down(k).start()

    def z_arrive(k):
        @pl.when(z - 1 - k >= 0)
        def _():
            b = block_of(z - 1 - k)
            remote(
                b, b, z_send.at[0, k], z_recv.at[0, k], {"sp": lax.rem(s + Y, S)}
            ).wait_recv()

        @pl.when(z + 1 + k <= Z - 1)
        def _():
            b = block_of(z + 1 + k)
            remote(
                b, b, z_send.at[1, k], z_recv.at[1, k], {"sp": lax.rem(s + S - Y, S)}
            ).wait_recv()

    if Z > 1:
        z_start(0)

    @pl.when(s < S - 1)
    def _():
        to_next.start()

    @pl.when(s > 0)
    def _():
        to_prev.start()

    loads[7].wait()
    loads[8].wait()

    @pl.loop(0, 2 * cols // TILE)
    def _(i):
        at = pl.ds(pl.multiple_of(i * TILE, TILE), TILE)
        wat = pl.ds(pl.multiple_of(2 * cols + i * TILE, TILE), TILE)
        qg[:, at] = dot(hid_lat[...], wall[:, wat]).astype(BF16)

    lane = lax.broadcasted_iota(jnp.int32, (GRID_W, 2 * GRID_W), 1) % GRID_W
    row = lax.broadcasted_iota(jnp.int32, (GRID_W, 2 * GRID_W), 0)
    first = jnp.clip(row - WIN_COLS // 2, 0, GRID_W - WIN_COLS)
    inside = (lane >= first) & (lane < first + WIN_COLS)
    pairs = table.shape[1]

    @pl.loop(0, heads)
    def _(h):
        for p in range(pairs):
            line = jnp.broadcast_to(table_rows[h, p : p + 1, :], (GRID_W, 2 * GRID_W))
            rolled = pltpu.roll(
                line, 2 * GRID_W - (WIN_COLS - 1), 1, stride=1, stride_axis=0
            )
            table[h, p] = jnp.where(inside, rolled, MASKED)

    for k in range(Z - 1):
        z_arrive(k)
        if k + 1 < Z - 1:
            z_start(k + 1)

    @pl.when(s > 0)
    def _():
        to_next.wait_recv()

    @pl.when(s < S - 1)
    def _():
        to_prev.wait_recv()

    total_rows = rows * S
    half = lax.broadcasted_iota(jnp.int32, (tokens, 128), 1) < 64
    scale = 0.125

    @pl.loop(0, heads // 2)
    def _(hp):
        at = pl.ds(pl.multiple_of(hp * 128, 128), 128)
        vat = pl.ds(pl.multiple_of(cols + hp * 128, 128), 128)
        q2 = qg[:, at].astype(F32) * scale
        ck = ckv[:, at]
        cv = ckv[:, vat]
        outs = []
        for e in range(2):
            q = jnp.where(half if e == 0 else jnp.logical_not(half), q2, 0.0).astype(BF16)
            sc = dot_t(q, ck)
            sw = []
            bands = []
            for r in range(rows):
                g = s * rows + r
                rs = jnp.clip(g - WIN_ROWS // 2, 0, total_rows - WIN_ROWS)
                band = pl.ds(
                    pl.multiple_of((rs - s * rows + rows) * GRID_W, GRID_W), WIN_ROWS * GRID_W
                )
                bands.append(band)
                bias = jnp.concatenate(
                    [
                        table[hp * 2 + e, rs - g + WIN_ROWS - 1 + 2 * p]
                        for p in range(WIN_ROWS // 2)
                    ],
                    axis=1,
                )
                sw.append(dot_t(q[r * GRID_W : (r + 1) * GRID_W], kv[band, at]) + bias)
            sw = jnp.concatenate(sw, axis=0)
            m = jnp.maximum(
                jnp.max(sc, axis=-1, keepdims=True), jnp.max(sw, axis=-1, keepdims=True)
            )
            pc = jnp.exp(sc - m)
            pw = jnp.exp(sw - m)
            total = jnp.sum(pc, axis=-1, keepdims=True) + jnp.sum(pw, axis=-1, keepdims=True)
            pw = pw.astype(BF16)
            o = dot(pc.astype(BF16), cv)
            ow = [
                dot(pw[r * GRID_W : (r + 1) * GRID_W], kv[bands[r], vat]) for r in range(rows)
            ]
            outs.append((o + jnp.concatenate(ow, axis=0)) / total)
        o = jnp.where(half, outs[0], outs[1])
        gate = qg[:, vat].astype(F32)
        gated[:, at] = (gate / (1.0 + jnp.exp(-gate)) * o).astype(BF16)

    loads[9].wait()
    own = tokens // T

    @pl.loop(0, width // TILE)
    def _(i):
        at = pl.ds(pl.multiple_of(i * TILE, TILE), TILE)
        prod[:, at] = dot(gated[...], wo[:, at]).astype(BF16)

    r_copies = []
    for d in range(1, T):
        other = lax.rem(t + d, T)
        copy = remote(
            prod.at[pl.ds(pl.multiple_of(other * own, own), own)],
            terms.at[d - 1],
            r_send.at[d - 1],
            r_recv.at[d - 1],
            {"tp": other},
        )
        copy.start()
        r_copies.append(copy)

    own_at = pl.ds(pl.multiple_of(t * own, own), own)
    total = prod[own_at, :].astype(F32)
    for i, copy in enumerate(r_copies):
        copy.wait()
        total = total + terms[i].astype(F32)
    b = total.astype(BF16).astype(F32)
    inv = lax.rsqrt(jnp.mean(b * b, axis=-1, keepdims=True) + EPSILON)
    out[...] = (
        lat[own_at, :].astype(F32) + modrow[4:5, :] * (b * inv * gain_post[...])
    ).astype(BF16)

    for k in range(Z - 1):

        @pl.when(send_up(k))
        def _():
            up(k).wait_send()

        @pl.when(send_down(k))
        def _():
            down(k).wait_send()

    @pl.when(s < S - 1)
    def _():
        to_next.wait_send()

    @pl.when(s > 0)
    def _():
        to_prev.wait_send()


def shards(
    S,
    T,
    latent,
    context,
    condition,
    context_condition,
    gain_pre,
    gain_post,
    w_shift,
    w_scale,
    w_gate,
    w_query,
    w_key,
    w_value,
    w_silu,
    offset_bias,
    w_out,
):
    in_rows, cols = w_shift.shape
    tokens, width = latent.shape
    n_ctx = context.shape[0]
    heads = offset_bias.shape[0]
    stacked = jnp.stack([condition, context_condition])
    own = lax.dynamic_slice_in_dim(stacked, lax.axis_index("sp") * in_rows, in_rows, 1)
    active = jnp.pad(jax.nn.silu(own.astype(F32)).astype(BF16), ((0, 14), (0, 0)))
    wide = jnp.pad(offset_bias, ((0, 0), (0, 0), (0, GRID_W - offset_bias.shape[2])))
    table_rows = jnp.concatenate([wide[:, :-1], wide[:, 1:]], axis=-1)
    pairs = table_rows.shape[1]
    own_rows = tokens // T
    vmem = pl.BlockSpec(memory_space=pltpu.VMEM)
    hbm = pl.BlockSpec(memory_space=pl.ANY)
    sem = pltpu.SemaphoreType.DMA
    Y = max(1, T // 2)
    if S % Y:
        Y = 1
    Z = S // Y
    return pl.pallas_call(
        functools.partial(kernel, S, T),
        out_shape=jax.ShapeDtypeStruct((own_rows, width), BF16),
        in_specs=[vmem] * 4 + [hbm] * 10,
        out_specs=vmem,
        scratch_shapes=[
            pltpu.VMEM((tokens, width), BF16),
            pltpu.VMEM((n_ctx, width), BF16),
            pltpu.VMEM((3, in_rows, cols), BF16),
            pltpu.VMEM((width, 4 * cols), BF16),
            pltpu.VMEM((cols, width), BF16),
            pltpu.VMEM((8, cols), F32),
            pltpu.VMEM((S, 8, cols), F32),
            pltpu.VMEM((T, 8, cols), F32),
            pltpu.VMEM((8, width), F32),
            pltpu.VMEM((tokens, width), F32),
            pltpu.VMEM((n_ctx, width), F32),
            pltpu.VMEM((tokens, width), BF16),
            pltpu.VMEM((n_ctx, width), BF16),
            pltpu.VMEM((tokens, 2 * cols), BF16),
            pltpu.VMEM((3 * tokens, 2 * cols), BF16),
            pltpu.VMEM((S * n_ctx, 2 * cols), BF16),
            pltpu.VMEM((heads, pairs, GRID_W, 2 * GRID_W), F32),
            pltpu.VMEM((tokens, cols), BF16),
            pltpu.VMEM((tokens, width), BF16),
            pltpu.VMEM((max(T - 1, 1), own_rows, width), BF16),
            sem((10,)),
            sem((max(S - 1, 1),)),
            sem((max(S - 1, 1),)),
            sem((max(T - 1, 1),)),
            sem((max(T - 1, 1),)),
            sem((max(Y - 1, 1),)),
            sem((max(Y - 1, 1),)),
            sem((2, max(Z - 1, 1))),
            sem((2, max(Z - 1, 1))),
            sem((2,)),
            sem((2,)),
            sem((max(T - 1, 1),)),
            sem((max(T - 1, 1),)),
        ],
        compiler_params=pltpu.CompilerParams(
            collective_id=0, has_side_effects=True, vmem_limit_bytes=60 * 1024 * 1024
        ),
    )(
        active,
        gain_pre.reshape(1, width),
        gain_post.reshape(1, width),
        table_rows,
        latent,
        context,
        w_shift,
        w_scale,
        w_gate,
        w_query,
        w_key,
        w_value,
        w_silu,
        w_out,
    )


def solution(mesh):
    in_specs = (
        P("sp", None),
        P("sp", None),
        P(),
        P(),
        P(),
        P(),
        P("sp", "tp"),
        P("sp", "tp"),
        P("sp", "tp"),
        P(None, "tp"),
        P(None, "tp"),
        P(None, "tp"),
        P(None, "tp"),
        P("tp", None, None),
        P("tp", None),
    )
    return jax.shard_map(
        functools.partial(shards, mesh.shape["sp"], mesh.shape["tp"]),
        mesh=mesh,
        in_specs=in_specs,
        out_specs=P(("sp", "tp"), None),
        check_vma=False,
    )
```

time: 196 us -> 96.9 us (0.49)
  Pallas kernels: 0 us -> 90.8 us
  local copies, waits for them, and re-layouts: 57.6 us -> 4.52 us
  blocking collectives: 44.1 us -> 0 us
  matrix products: 31.8 us -> 0 us
  waiting for transfers between devices: 22.2 us -> 0 us
  other arithmetic: 18.6 us -> 0.81 us
  between operations: 13.8 us -> 0.02 us
  starting transfers between devices: 6.83 us -> 0 us
    pallas_call x0 -> x1, Pallas kernels: none -> 90.8 us  [shards(): pl.pallas_call(functools.partial(kernel, S, T), out_shape=jax.ShapeDtypeS...]
    psum x1 -> x0, blocking collectives: 38.9 us -> none  [shards(): summed = lax.psum(partial_value, 'sp')]
    gather x2 -> x0, local copies, waits for them, and re-layouts: 33.9 us -> none  [shards(): jnp.take(flat_rows, position.reshape(-1), axis=0)]
    dot_general x13 -> x0, matrix products: 31.8 us -> none  [the longest x6 9.43 us: product(): return jnp.dot(left, right, preferred_element_type=jnp.float32)]
    reduce_scatter x1 -> x0, waiting for transfers between devices: 22.2 us -> none  [shards(): lax.psum_scatter(product(gated_heads, w_out).astype(jnp.bfloat16), 'tp',...]
    slice x4 -> x1, local copies, waits for them, and re-layouts: 12.8 us -> 0.01 us  [shards(): table_rows = jnp.concatenate([wide[:, :-1], wide[:, 1:]], axis=-1)]
    reshape x3 -> x0, local copies, waits for them, and re-layouts: 8.71 us -> none  [the longest x1 7.36 us: shards(): offset_terms = jnp.einsum('rva,hbqwa->rbhqvw', row_table, by_column, prec...]
    select_n x2 -> x0, other arithmetic: 7.45 us -> none  [shards(): jnp.take(flat_rows, position.reshape(-1), axis=0)]
  transfers between devices with their start and end apart: 4 -> 0, of which waited for: 1 -> 0; matrix products, arithmetic and copies ran while one was open for 38% -> 0% of each run, Pallas kernels for 0% -> 0%
where the time goes in v1:
time: 96.9 us; the launch traced here: 96.2 us
  Pallas kernels  90.8 us (94%)
  local copies, waits for them, and re-layouts  4.52 us (5%)
    pallas_call x1, Pallas kernels, shards(): pl.pallas_call(functools.partial(kernel, S, T), out_shape=jax.ShapeDtypeS...  90.8 us
    unnamed x2, local copies, waits for them, and re-layouts  2.51 us

profile of v1, /device:TPU:0, one launch (start us, length us, event | category | flops | bytes accessed | tf_op | source)
XLA Modules:
  0.0 96.2 jit_solution(15422356935498084534)
XLA Ops:
  0.0 0.7 stack.9
  0.7 0.7 stack.10
  1.4 0.1 fusion.2
  1.5 0.6 pad.8.active
  2.1 0.8 copy.16
  3.0 0.7 pad_maximum_fusion.table_rows
  3.7 90.8 %shard_map.145 = bf16[64,2048]{1,0:T(8,128)(2,1)} custom-call(bf16[16,256]{1,0:T(8,128)(2,1)} %pad.8.active, f32[1,2048]{1,0:T(1,128)} %bitcast.2, f32[1,2048]{1,0:T(1,128)} %bitcast.3, f32[8,14,128]{2,1,0:T(8,128)} %pad_maximum_fusion.table_rows, bf16[256,2048]{1,0:T(8,128)(2,1)} %latent_hbm.1, bf16[128,2048]{1,0:T(8,128)(2,1)} %context_hbm.1, ...), custom_call_target="tpu_custom_call" | custom-call | tf_op jit(solution)/shard_map/pallas_call | solution.py:475
  94.5 1.7 %copy.18 = bf16[64,2048]{1,0:T(8,128)(2,1)} copy(bf16[64,2048]{1,0:T(8,128)(2,1)} %shard_map.145) | data formatting | bytes 524288
  (1 shorter events, 0.0 us)

commit v2 on v1

v2 whole, which is shorter than its diff:
```python
import functools

import jax
import jax.numpy as jnp
from jax import lax
from jax.experimental import pallas as pl
from jax.experimental.pallas import tpu as pltpu
from jax.sharding import PartitionSpec as P

GRID_W = 64
WIN_ROWS = 8
WIN_COLS = 16
EPSILON = 1e-06
MASKED = -1e30
F32 = jnp.float32
BF16 = jnp.bfloat16
TILE = 256


def remote(src, dst, send, recv, where):
    return pltpu.make_async_remote_copy(
        src_ref=src,
        dst_ref=dst,
        send_sem=send,
        recv_sem=recv,
        device_id=where,
        device_id_type=pl.DeviceIdType.MESH,
    )


def dot(a, b):
    return jnp.dot(a, b, preferred_element_type=F32)


def dot_t(a, b):
    return lax.dot_general(a, b, (((1,), (1,)), ((), ())), preferred_element_type=F32)


def kernel(
    S,
    T,
    active,
    gain_pre,
    gain_post,
    table_rows,
    latent_hbm,
    context_hbm,
    wsh_hbm,
    wsc_hbm,
    wga_hbm,
    wq_hbm,
    wk_hbm,
    wv_hbm,
    ws_hbm,
    wo_hbm,
    out,
    lat,
    ctx,
    wmod,
    wall,
    wo,
    part,
    modbuf,
    modfull,
    modrow,
    hid,
    qg,
    kv,
    ckv,
    table,
    gated,
    prod,
    pair,
    mate,
    terms,
    load_sem,
    a_send,
    a_recv,
    b_send,
    b_recv,
    y_send,
    y_recv,
    z_send,
    z_recv,
    x_send,
    x_recv,
    d_send,
    d_recv,
    h_send,
    h_recv,
    m_send,
    m_recv,
    r_send,
    r_recv,
):
    s = lax.axis_index("sp")
    t = lax.axis_index("tp")
    width = lat.shape[1]
    tokens = lat.shape[0] // 3
    n_ctx = ctx.shape[0] // S
    cols = wo.shape[0]
    heads = table.shape[0]
    rows = tokens // GRID_W
    X, Y, Z = layout_of(S, T)
    z = s // Y
    y = s % Y
    xi = t // 2
    core = t % 2
    partner = {"tp": t + 1 - 2 * core}
    half_width = width // 2
    slice_width = width // T
    own_lat = pl.ds(tokens, tokens)

    def ctx_rows(b):
        return pl.ds(pl.multiple_of(b * n_ctx, n_ctx), n_ctx)

    def ctx_slice(b, j):
        return ctx.at[ctx_rows(b), pl.ds(pl.multiple_of(j * slice_width, slice_width), slice_width)]

    loads = []
    for i, (src, dst) in enumerate(
        [
            (context_hbm, ctx.at[ctx_rows(s)]),
            (wsh_hbm, wmod.at[0]),
            (wsc_hbm, wmod.at[1]),
            (wga_hbm, wmod.at[2]),
            (latent_hbm, lat.at[own_lat]),
            (wk_hbm, wall.at[:, pl.ds(0, cols)]),
            (wv_hbm, wall.at[:, pl.ds(cols, cols)]),
            (wq_hbm, wall.at[:, pl.ds(2 * cols, cols)]),
            (ws_hbm, wall.at[:, pl.ds(3 * cols, cols)]),
            (wo_hbm, wo),
        ]
    ):
        copy = pltpu.make_async_copy(src, dst, load_sem.at[i])
        copy.start()
        loads.append(copy)

    barrier = pltpu.get_barrier_semaphore()
    for d in range(1, S):
        pl.semaphore_signal(
            barrier, inc=1, device_id={"sp": lax.rem(s + d, S)}, device_id_type=pl.DeviceIdType.MESH
        )
    for d in range(1, T):
        pl.semaphore_signal(
            barrier, inc=1, device_id={"tp": lax.rem(t + d, T)}, device_id_type=pl.DeviceIdType.MESH
        )

    pending = []

    def send(cond, copy):
        pending.append((cond, copy))
        if cond is None:
            copy.start()
        else:

            @pl.when(cond)
            def _():
                copy.start()

    def arrive(cond, copy):
        if cond is None:
            copy.wait_recv()
        else:

            @pl.when(cond)
            def _():
                copy.wait_recv()

    part[...] = jnp.zeros_like(part)
    loads[0].wait()
    pl.semaphore_wait(barrier, S - 1 + T - 1)

    for d in range(1, Y):
        send(
            None,
            remote(
                ctx_slice(s, t),
                ctx_slice(s, t),
                y_send.at[d - 1],
                y_recv.at[d - 1],
                {"sp": z * Y + lax.rem(y + d, Y)},
            ),
        )

    for i in range(3):
        loads[1 + i].wait()
        part[2 * i : 2 * i + 2, :] = dot(active[...], wmod[i])[0:2]

    a_copies = []
    for d in range(1, S):
        copy = remote(
            part, modbuf.at[s], a_send.at[d - 1], a_recv.at[d - 1], {"sp": lax.rem(s + d, S)}
        )
        copy.start()
        a_copies.append(copy)

    loads[4].wait()

    def lat_part(where, side):
        return lat.at[
            pl.ds(where * tokens, tokens),
            pl.ds(pl.multiple_of(side * half_width, half_width), half_width),
        ]

    to_next = remote(
        lat_part(1, core), lat_part(0, core), h_send.at[0], h_recv.at[0], {"sp": lax.rem(s + 1, S)}
    )
    to_prev = remote(
        lat_part(1, core),
        lat_part(2, core),
        h_send.at[1],
        h_recv.at[1],
        {"sp": lax.rem(s + S - 1, S)},
    )
    send(s < S - 1, to_next)
    send(s > 0, to_prev)

    def units_of(k):
        if k < 0:
            return [(d - 1, z * Y + lax.rem(y + Y - d, Y), None) for d in range(1, Y)]
        units = []
        for way in range(2):
            at = z - 1 - k if way == 0 else z + 1 + k
            have = at >= 0 if way == 0 else at <= Z - 1
            for u in range(Y):
                units.append((Y - 1 + (k * 2 + way) * Y + u, at * Y + u, have))
        return units

    def chain(way, k, u):
        at = z - k if way == 0 else z + k
        have = ((at >= 0) & (z < Z - 1)) if way == 0 else ((at <= Z - 1) & (z > 0))
        target = lax.rem(s + Y, S) if way == 0 else lax.rem(s + S - Y, S)
        b = ctx_slice(at * Y + u, t)
        return have, remote(b, b, z_send.at[way, k, u], z_recv.at[way, k, u], {"sp": target})

    def chain_start(k):
        if k < Z - 1:
            for u in range(Y):
                for way in range(2):
                    send(*chain(way, k, u))

    def share(unit):
        n, b, have = unit
        mine = ctx_slice(b, t)
        for d in range(1, X):
            send(
                have,
                remote(
                    mine,
                    mine,
                    x_send.at[n * (X - 1) + d - 1] if X > 1 else None,
                    x_recv.at[n * (X - 1) + d - 1] if X > 1 else None,
                    {"tp": lax.rem(xi + d, X) * 2 + core},
                ),
            )
        send(have, remote(mine, mine, d_send.at[n * X], d_recv.at[n * X], partner))

    def own_arrive(k):
        if k < 0:
            for d in range(1, Y):
                b = ctx_slice(z * Y + lax.rem(y + Y - d, Y), t)
                arrive(None, remote(b, b, y_send.at[d - 1], y_recv.at[d - 1], partner))
        else:
            for n, b, have in units_of(k):
                way, u = ((n - (Y - 1)) // Y) % 2, (n - (Y - 1)) % Y
                ref = ctx_slice(b, t)
                arrive(
                    have,
                    remote(ref, ref, z_send.at[way, k, u], z_recv.at[way, k, u], partner),
                )
        chain_start(k + 1)
        for unit in units_of(k):
            share(unit)

    def x_arrive(k):
        for n, b, have in units_of(k):
            for d in range(1, X):
                ref = ctx_slice(b, lax.rem(xi + X - d, X) * 2 + core)
                at = n * (X - 1) + d - 1
                arrive(have, remote(ref, ref, x_send.at[at], x_recv.at[at], partner))
                send(
                    have, remote(ref, ref, d_send.at[n * X + d], d_recv.at[n * X + d], partner)
                )

    def mate_arrive(k):
        for n, b, have in units_of(k):
            for d in range(X):
                ref = ctx_slice(b, lax.rem(xi + X - d, X) * 2 + 1 - core)
                arrive(have, remote(ref, ref, d_send.at[n * X + d], d_recv.at[n * X + d], partner))

    def hidden(src, first, count, kind):
        step = 32

        @pl.loop(0, count // step)
        def _(i):
            at = pl.ds(pl.multiple_of(first + i * step, step), step)
            v = src[at, :].astype(F32)
            inv = lax.rsqrt(jnp.mean(v * v, axis=-1, keepdims=True) + EPSILON)
            v = v * inv * modrow[2 + kind : 3 + kind, :] + modrow[kind : kind + 1, :]
            hid[pl.ds(pl.multiple_of(i * step, step), step), :] = v.astype(BF16)

    def project(count, dst, first, tiles, start):
        @pl.loop(0, tiles)
        def _(i):
            at = pl.ds(pl.multiple_of(i * TILE, TILE), TILE)
            wat = pl.ds(pl.multiple_of(start + i * TILE, TILE), TILE)
            dst[pl.ds(first, count), at] = dot(hid[0:count, :], wall[:, wat]).astype(BF16)

    def ctx_project(at):
        count = Y * n_ctx
        first = pl.multiple_of(at * count, count)
        hidden(ctx, first, count, 1)
        project(count, ckv, first, 2 * cols // TILE, 0)

    def process(k):
        mate_arrive(k)
        if k < 0:
            ctx_project(z)
        else:

            @pl.when(z - 1 - k >= 0)
            def _():
                ctx_project(z - 1 - k)

            @pl.when(z + 1 + k <= Z - 1)
            def _():
                ctx_project(z + 1 + k)

    own_arrive(-1)

    lane = lax.broadcasted_iota(jnp.int32, (GRID_W, 2 * GRID_W), 1) % GRID_W
    row = lax.broadcasted_iota(jnp.int32, (GRID_W, 2 * GRID_W), 0)
    first = jnp.clip(row - WIN_COLS // 2, 0, GRID_W - WIN_COLS)
    inside = (lane >= first) & (lane < first + WIN_COLS)
    pairs = table.shape[1]

    @pl.loop(0, heads)
    def _(h):
        for p in range(pairs):
            line = jnp.broadcast_to(table_rows[h, p : p + 1, :], (GRID_W, 2 * GRID_W))
            rolled = pltpu.roll(
                line, 2 * GRID_W - (WIN_COLS - 1), 1, stride=1, stride_axis=0
            )
            table[h, p] = jnp.where(inside, rolled, MASKED)

    modbuf[s] = part[...]
    for copy in a_copies:
        copy.wait()
    modfull[t] = jnp.sum(modbuf[...], axis=0)
    b_copies = []
    for d in range(1, T):
        copy = remote(
            modfull.at[t],
            modfull.at[t],
            b_send.at[d - 1],
            b_recv.at[d - 1],
            {"tp": lax.rem(t + d, T)},
        )
        copy.start()
        b_copies.append(copy)

    x_arrive(-1)
    if Z > 1:
        own_arrive(0)
    for copy in b_copies:
        copy.wait()
    for j in range(T):
        at = slice(j * cols, (j + 1) * cols)
        modrow[:, at] = modfull[j]
        modrow[2:4, at] = gain_pre[:, at] * (1.0 + modfull[j, 2:4])

    for i in range(5, 9):
        loads[i].wait()
    hidden(lat, tokens, tokens, 0)
    project(tokens, kv, tokens, 2 * cols // TILE, 0)
    project(tokens, qg, 0, 2 * cols // TILE, 2 * cols)

    def halo_share():
        arrive(s > 0, to_next)
        send(
            s > 0,
            remote(lat_part(0, core), lat_part(0, core), m_send.at[0], m_recv.at[0], partner),
        )
        arrive(s < S - 1, to_prev)
        send(
            s < S - 1,
            remote(lat_part(2, core), lat_part(2, core), m_send.at[1], m_recv.at[1], partner),
        )

    for k in range(1, Z - 1):
        own_arrive(k)
        x_arrive(k - 1)
        process(k - 2)
    if Z > 1:
        x_arrive(Z - 2)
        if Z > 2:
            process(Z - 3)
    halo_share()
    if Z > 1:
        process(Z - 2)
    else:
        process(-1)

    @pl.when(s > 0)
    def _():
        ref = lat_part(0, 1 - core)
        remote(ref, ref, m_send.at[0], m_recv.at[0], partner).wait_recv()
        hidden(lat, 0, tokens, 0)
        project(tokens, kv, 0, 2 * cols // TILE, 0)

    @pl.when(s < S - 1)
    def _():
        ref = lat_part(2, 1 - core)
        remote(ref, ref, m_send.at[1], m_recv.at[1], partner).wait_recv()
        hidden(lat, 2 * tokens, tokens, 0)
        project(tokens, kv, 2 * tokens, 2 * cols // TILE, 0)

    total_rows = rows * S
    half = lax.broadcasted_iota(jnp.int32, (tokens, 128), 1) < 64
    scale = 0.125

    @pl.loop(0, heads // 2)
    def _(hp):
        at = pl.ds(pl.multiple_of(hp * 128, 128), 128)
        vat = pl.ds(pl.multiple_of(cols + hp * 128, 128), 128)
        q2 = qg[:, at].astype(F32) * scale
        ck = ckv[:, at]
        cv = ckv[:, vat]
        outs = []
        for e in range(2):
            q = jnp.where(half if e == 0 else jnp.logical_not(half), q2, 0.0).astype(BF16)
            sc = dot_t(q, ck)
            sw = []
            bands = []
            for r in range(rows):
                g = s * rows + r
                rs = jnp.clip(g - WIN_ROWS // 2, 0, total_rows - WIN_ROWS)
                band = pl.ds(
                    pl.multiple_of((rs - s * rows + rows) * GRID_W, GRID_W), WIN_ROWS * GRID_W
                )
                bands.append(band)
                bias = jnp.concatenate(
                    [
                        table[hp * 2 + e, rs - g + WIN_ROWS - 1 + 2 * p]
                        for p in range(WIN_ROWS // 2)
                    ],
                    axis=1,
                )
                sw.append(dot_t(q[r * GRID_W : (r + 1) * GRID_W], kv[band, at]) + bias)
            sw = jnp.concatenate(sw, axis=0)
            m = jnp.maximum(
                jnp.max(sc, axis=-1, keepdims=True), jnp.max(sw, axis=-1, keepdims=True)
            )
            pc = jnp.exp(sc - m)
            pw = jnp.exp(sw - m)
            total = jnp.sum(pc, axis=-1, keepdims=True) + jnp.sum(pw, axis=-1, keepdims=True)
            pw = pw.astype(BF16)
            o = dot(pc.astype(BF16), cv)
            ow = [
                dot(pw[r * GRID_W : (r + 1) * GRID_W], kv[bands[r], vat]) for r in range(rows)
            ]
            outs.append((o + jnp.concatenate(ow, axis=0)) / total)
        o = jnp.where(half, outs[0], outs[1])
        gate = qg[:, vat].astype(F32)
        gated[:, at] = (gate / (1.0 + jnp.exp(-gate)) * o).astype(BF16)

    loads[9].wait()
    own = tokens // T
    groups = 4
    span = width // groups
    m_copies = []
    for g in range(groups):
        span_at = pl.ds(g * span, span)
        prod[:, span_at] = dot(gated[...], wo[:, span_at]).astype(BF16)
        copies = []
        for i in range(X):
            n = g * X + i
            copy = remote(
                prod.at[
                    pl.ds(pl.multiple_of((i * 2 + 1 - core) * own, own), own), span_at
                ],
                mate.at[i, :, span_at],
                m_send.at[2 + n],
                m_recv.at[2 + n],
                partner,
            )
            copy.start()
            copies.append(copy)
        m_copies.append(copies)
    r_copies = []
    for g in range(groups):
        span_at = pl.ds(g * span, span)
        for copy in m_copies[g]:
            copy.wait()
        copies = []
        for i in range(X):
            at = pl.ds(pl.multiple_of((i * 2 + core) * own, own), own)
            pair[i, :, span_at] = (
                prod[at, span_at].astype(F32) + mate[i, :, span_at].astype(F32)
            )
            if X > 1:
                prod[at, span_at] = pair[i, :, span_at].astype(BF16)
        for d in range(1, X):
            other = lax.rem(xi + d, X)
            n = g * (X - 1) + d - 1
            copy = remote(
                prod.at[pl.ds(pl.multiple_of((other * 2 + core) * own, own), own), span_at],
                terms.at[d - 1, :, span_at],
                r_send.at[n],
                r_recv.at[n],
                {"tp": other * 2 + core},
            )
            copy.start()
            copies.append(copy)
        r_copies.append(copies)
    for copies in r_copies:
        for copy in copies:
            copy.wait()
    total = pair[xi]
    for d in range(1, X):
        total = total + terms[d - 1].astype(F32)
    b = total.astype(BF16).astype(F32)
    inv = lax.rsqrt(jnp.mean(b * b, axis=-1, keepdims=True) + EPSILON)
    own_at = pl.ds(pl.multiple_of(tokens + t * own, own), own)
    out[...] = (
        lat[own_at, :].astype(F32) + modrow[4:5, :] * (b * inv * gain_post[...])
    ).astype(BF16)

    for cond, copy in pending:
        if cond is None:
            copy.wait_send()
        else:

            @pl.when(cond)
            def _(copy=copy):
                copy.wait_send()


def layout_of(S, T):
    X = T // 2
    Y = X if S % X == 0 else 1
    return X, Y, S // Y


def shards(
    S,
    T,
    latent,
    context,
    condition,
    context_condition,
    gain_pre,
    gain_post,
    w_shift,
    w_scale,
    w_gate,
    w_query,
    w_key,
    w_value,
    w_silu,
    offset_bias,
    w_out,
):
    in_rows, cols = w_shift.shape
    tokens, width = latent.shape
    n_ctx = context.shape[0]
    heads = offset_bias.shape[0]
    stacked = jnp.stack([condition, context_condition])
    own = lax.dynamic_slice_in_dim(stacked, lax.axis_index("sp") * in_rows, in_rows, 1)
    active = jnp.pad(jax.nn.silu(own.astype(F32)).astype(BF16), ((0, 14), (0, 0)))
    wide = jnp.pad(offset_bias, ((0, 0), (0, 0), (0, GRID_W - offset_bias.shape[2])))
    table_rows = jnp.concatenate([wide[:, :-1], wide[:, 1:]], axis=-1)
    pairs = table_rows.shape[1]
    own_rows = tokens // T
    vmem = pl.BlockSpec(memory_space=pltpu.VMEM)
    hbm = pl.BlockSpec(memory_space=pl.ANY)
    sem = pltpu.SemaphoreType.DMA
    X, Y, Z = layout_of(S, T)
    units = Y - 1 + 2 * (Z - 1) * Y
    return pl.pallas_call(
        functools.partial(kernel, S, T),
        out_shape=jax.ShapeDtypeStruct((own_rows, width), BF16),
        in_specs=[vmem] * 4 + [hbm] * 10,
        out_specs=vmem,
        scratch_shapes=[
            pltpu.VMEM((3 * tokens, width), BF16),
            pltpu.VMEM((S * n_ctx, width), BF16),
            pltpu.VMEM((3, in_rows, cols), BF16),
            pltpu.VMEM((width, 4 * cols), BF16),
            pltpu.VMEM((cols, width), BF16),
            pltpu.VMEM((8, cols), F32),
            pltpu.VMEM((S, 8, cols), F32),
            pltpu.VMEM((T, 8, cols), F32),
            pltpu.VMEM((8, width), F32),
            pltpu.VMEM((max(tokens, Y * n_ctx), width), BF16),
            pltpu.VMEM((tokens, 2 * cols), BF16),
            pltpu.VMEM((3 * tokens, 2 * cols), BF16),
            pltpu.VMEM((S * n_ctx, 2 * cols), BF16),
            pltpu.VMEM((heads, pairs, GRID_W, 2 * GRID_W), F32),
            pltpu.VMEM((tokens, cols), BF16),
            pltpu.VMEM((tokens, width), BF16),
            pltpu.VMEM((X, own_rows, width), F32),
            pltpu.VMEM((X, own_rows, width), BF16),
            pltpu.VMEM((max(X - 1, 1), own_rows, width), BF16),
            sem((10,)),
            sem((max(S - 1, 1),)),
            sem((max(S - 1, 1),)),
            sem((max(T - 1, 1),)),
            sem((max(T - 1, 1),)),
            sem((max(Y - 1, 1),)),
            sem((max(Y - 1, 1),)),
            sem((2, max(Z - 1, 1), Y)),
            sem((2, max(Z - 1, 1), Y)),
            sem((max(units * (X - 1), 1),)),
            sem((max(units * (X - 1), 1),)),
            sem((max(units * X, 1),)),
            sem((max(units * X, 1),)),
            sem((2,)),
            sem((2,)),
            sem((2 + 4 * X,)),
            sem((2 + 4 * X,)),
            sem((4 * max(X - 1, 1),)),
            sem((4 * max(X - 1, 1),)),
        ],
        compiler_params=pltpu.CompilerParams(
            collective_id=0, has_side_effects=True, vmem_limit_bytes=60 * 1024 * 1024
        ),
    )(
        active,
        gain_pre.reshape(1, width),
        gain_post.reshape(1, width),
        table_rows,
        latent,
        context,
        w_shift,
        w_scale,
        w_gate,
        w_query,
        w_key,
        w_value,
        w_silu,
        w_out,
    )


def solution(mesh):
    in_specs = (
        P("sp", None),
        P("sp", None),
        P(),
        P(),
        P(),
        P(),
        P("sp", "tp"),
        P("sp", "tp"),
        P("sp", "tp"),
        P(None, "tp"),
        P(None, "tp"),
        P(None, "tp"),
        P(None, "tp"),
        P("tp", None, None),
        P("tp", None),
    )
    return jax.shard_map(
        functools.partial(shards, mesh.shape["sp"], mesh.shape["tp"]),
        mesh=mesh,
        in_specs=in_specs,
        out_specs=P(("sp", "tp"), None),
        check_vma=False,
    )
```

time: 96.9 us -> 86.3 us (0.89)
  the two profiles are of different devices: /device:TPU:0 before, /device:TPU:16 now
where the time goes in v2:
time: 86.3 us; the launch traced here: 86 us
  Pallas kernels  80.6 us (93%)
  local copies, waits for them, and re-layouts  4.52 us (5%)
    pallas_call x1, Pallas kernels, shards(): pl.pallas_call(functools.partial(kernel, S, T), out_shape=jax.ShapeDtypeS...  80.6 us
    unnamed x2, local copies, waits for them, and re-layouts  2.51 us

profile of v2, /device:TPU:16, one launch (start us, length us, event | category | flops | bytes accessed | tf_op | source)
XLA Modules:
  0.0 86.0 jit_solution(8291870527799702110)
XLA Ops:
  0.0 0.7 stack.9
  0.7 0.7 stack.10
  1.4 0.1 fusion.2
  1.5 0.6 pad.8.active
  2.1 0.8 copy.16
  3.0 0.7 pad_maximum_fusion.table_rows
  3.7 80.6 %shard_map.145 = bf16[64,2048]{1,0:T(8,128)(2,1)} custom-call(bf16[16,256]{1,0:T(8,128)(2,1)} %pad.8.active, f32[1,2048]{1,0:T(1,128)} %bitcast.2, f32[1,2048]{1,0:T(1,128)} %bitcast.3, f32[8,14,128]{2,1,0:T(8,128)} %pad_maximum_fusion.table_rows, bf16[256,2048]{1,0:T(8,128)(2,1)} %latent_hbm.1, bf16[128,2048]{1,0:T(8,128)(2,1)} %context_hbm.1, ...), custom_call_target="tpu_custom_call" | custom-call | tf_op jit(solution)/shard_map/pallas_call | solution.py:581
  84.3 1.7 %copy.18 = bf16[64,2048]{1,0:T(8,128)(2,1)} copy(bf16[64,2048]{1,0:T(8,128)(2,1)} %shard_map.145) | data formatting | bytes 524288
  (1 shorter events, 0.0 us)

commit v3 on v2

--- a/solution.py
+++ b/solution.py
@@ -14,7 +14,8 @@
 MASKED = -1e30
 F32 = jnp.float32
 BF16 = jnp.bfloat16
-TILE = 256
+TILE = 512
+PIECES = 4
 
 
 def remote(src, dst, send, recv, where):
@@ -183,6 +184,17 @@
             ),
         )
 
+    def chain(way, k, u):
+        at = z - k if way == 0 else z + k
+        have = ((at >= 0) & (z < Z - 1)) if way == 0 else ((at <= Z - 1) & (z > 0))
+        target = lax.rem(s + Y, S) if way == 0 else lax.rem(s + S - Y, S)
+        b = ctx_slice(at * Y + lax.rem(y + u, Y), t)
+        return have, remote(b, b, z_send.at[way, k, u], z_recv.at[way, k, u], {"sp": target})
+
+    for way in range(2):
+        if Z > 1:
+            send(*chain(way, 0, 0))
+
     for i in range(3):
         loads[1 + i].wait()
         part[2 * i : 2 * i + 2, :] = dot(active[...], wmod[i])[0:2]
@@ -197,24 +209,37 @@
 
     loads[4].wait()
 
-    def lat_part(where, side):
+    piece = half_width // PIECES
+
+    def lat_part(where, side, p):
         return lat.at[
             pl.ds(where * tokens, tokens),
-            pl.ds(pl.multiple_of(side * half_width, half_width), half_width),
+            pl.ds(pl.multiple_of(side * half_width + p * piece, piece), piece),
         ]
 
-    to_next = remote(
-        lat_part(1, core), lat_part(0, core), h_send.at[0], h_recv.at[0], {"sp": lax.rem(s + 1, S)}
-    )
-    to_prev = remote(
-        lat_part(1, core),
-        lat_part(2, core),
-        h_send.at[1],
-        h_recv.at[1],
-        {"sp": lax.rem(s + S - 1, S)},
-    )
-    send(s < S - 1, to_next)
-    send(s > 0, to_prev)
+    def to_next(p):
+        return remote(
+            lat_part(1, core, p),
+            lat_part(0, core, p),
+            h_send.at[0, p],
+            h_recv.at[0, p],
+            {"sp": lax.rem(s + 1, S)},
+        )
+
+    def to_prev(p):
+        return remote(
+            lat_part(1, core, p),
+            lat_part(2, core, p),
+            h_send.at[1, p],
+            h_recv.at[1, p],
+            {"sp": lax.rem(s + S - 1, S)},
+        )
+
+    def halo_start(p):
+        send(s < S - 1, to_next(p))
+        send(s > 0, to_prev(p))
+
+    halo_start(0)
 
     def units_of(k):
         if k < 0:
@@ -224,21 +249,8 @@
             at = z - 1 - k if way == 0 else z + 1 + k
             have = at >= 0 if way == 0 else at <= Z - 1
             for u in range(Y):
-                units.append((Y - 1 + (k * 2 + way) * Y + u, at * Y + u, have))
+                units.append((Y - 1 + (k * 2 + way) * Y + u, at * Y + lax.rem(y + u, Y), have))
         return units
-
-    def chain(way, k, u):
-        at = z - k if way == 0 else z + k
-        have = ((at >= 0) & (z < Z - 1)) if way == 0 else ((at <= Z - 1) & (z > 0))
-        target = lax.rem(s + Y, S) if way == 0 else lax.rem(s + S - Y, S)
-        b = ctx_slice(at * Y + u, t)
-        return have, remote(b, b, z_send.at[way, k, u], z_recv.at[way, k, u], {"sp": target})
-
-    def chain_start(k):
-        if k < Z - 1:
-            for u in range(Y):
-                for way in range(2):
-                    send(*chain(way, k, u))
 
     def share(unit):
         n, b, have = unit
@@ -257,21 +269,23 @@
         send(have, remote(mine, mine, d_send.at[n * X], d_recv.at[n * X], partner))
 
     def own_arrive(k):
-        if k < 0:
-            for d in range(1, Y):
-                b = ctx_slice(z * Y + lax.rem(y + Y - d, Y), t)
-                arrive(None, remote(b, b, y_send.at[d - 1], y_recv.at[d - 1], partner))
-        else:
-            for n, b, have in units_of(k):
+        for n, b, have in units_of(k):
+            ref = ctx_slice(b, t)
+            if k < 0:
+                arrive(None, remote(ref, ref, y_send.at[n], y_recv.at[n], partner))
+                u = Y - 1 - n
+                if Z > 1:
+                    send(*chain(0, 0, u))
+                    send(*chain(1, 0, u))
+            else:
                 way, u = ((n - (Y - 1)) // Y) % 2, (n - (Y - 1)) % Y
-                ref = ctx_slice(b, t)
                 arrive(
                     have,
                     remote(ref, ref, z_send.at[way, k, u], z_recv.at[way, k, u], partner),
                 )
-        chain_start(k + 1)
-        for unit in units_of(k):
-            share(unit)
+                if k + 1 < Z - 1:
+                    send(*chain(way, k + 1, u))
+            share((n, b, have))
 
     def x_arrive(k):
         for n, b, have in units_of(k):
@@ -292,7 +306,7 @@
     def hidden(src, first, count, kind):
         step = 32
 
-        @pl.loop(0, count // step)
+        @pl.loop(0, count // step, unroll=min(4, count // step))
         def _(i):
             at = pl.ds(pl.multiple_of(first + i * step, step), step)
             v = src[at, :].astype(F32)
@@ -328,6 +342,7 @@
                 ctx_project(z + 1 + k)
 
     own_arrive(-1)
+    halo_start(1)
 
     lane = lax.broadcasted_iota(jnp.int32, (GRID_W, 2 * GRID_W), 1) % GRID_W
     row = lax.broadcasted_iota(jnp.int32, (GRID_W, 2 * GRID_W), 0)
@@ -360,9 +375,10 @@
         copy.start()
         b_copies.append(copy)
 
-    x_arrive(-1)
     if Z > 1:
         own_arrive(0)
+    halo_start(2)
+    x_arrive(-1)
     for copy in b_copies:
         copy.wait()
     for j in range(T):
@@ -374,22 +390,24 @@
         loads[i].wait()
     hidden(lat, tokens, tokens, 0)
     project(tokens, kv, tokens, 2 * cols // TILE, 0)
+    if Z > 2:
+        own_arrive(1)
+    halo_start(3)
     project(tokens, qg, 0, 2 * cols // TILE, 2 * cols)
 
     def halo_share():
-        arrive(s > 0, to_next)
-        send(
-            s > 0,
-            remote(lat_part(0, core), lat_part(0, core), m_send.at[0], m_recv.at[0], partner),
-        )
-        arrive(s < S - 1, to_prev)
-        send(
-            s < S - 1,
-            remote(lat_part(2, core), lat_part(2, core), m_send.at[1], m_recv.at[1], partner),
-        )
+        for p in range(PIECES):
+            arrive(s > 0, to_next(p))
+            mine = lat_part(0, core, p)
+            send(s > 0, remote(mine, mine, m_send.at[p], m_recv.at[p], partner))
+            arrive(s < S - 1, to_prev(p))
+            mine = lat_part(2, core, p)
+            n = PIECES + p
+            send(s < S - 1, remote(mine, mine, m_send.at[n], m_recv.at[n], partner))
 
     for k in range(1, Z - 1):
-        own_arrive(k)
+        if k > 1:
+            own_arrive(k)
         x_arrive(k - 1)
         process(k - 2)
     if Z > 1:
@@ -404,15 +422,17 @@
 
     @pl.when(s > 0)
     def _():
-        ref = lat_part(0, 1 - core)
-        remote(ref, ref, m_send.at[0], m_recv.at[0], partner).wait_recv()
+        for p in range(PIECES):
+            ref = lat_part(0, 1 - core, p)
+            remote(ref, ref, m_send.at[p], m_recv.at[p], partner).wait_recv()
         hidden(lat, 0, tokens, 0)
         project(tokens, kv, 0, 2 * cols // TILE, 0)
 
     @pl.when(s < S - 1)
     def _():
-        ref = lat_part(2, 1 - core)
-        remote(ref, ref, m_send.at[1], m_recv.at[1], partner).wait_recv()
+        for p in range(PIECES):
+            ref = lat_part(2, 1 - core, p)
+            remote(ref, ref, m_send.at[PIECES + p], m_recv.at[PIECES + p], partner).wait_recv()
         hidden(lat, 2 * tokens, tokens, 0)
         project(tokens, kv, 2 * tokens, 2 * cols // TILE, 0)
 
@@ -481,8 +501,8 @@
                     pl.ds(pl.multiple_of((i * 2 + 1 - core) * own, own), own), span_at
                 ],
                 mate.at[i, :, span_at],
-                m_send.at[2 + n],
-                m_recv.at[2 + n],
+                m_send.at[2 * PIECES + n],
+                m_recv.at[2 * PIECES + n],
                 partner,
             )
             copy.start()
@@ -616,10 +636,10 @@
             sem((max(units * (X - 1), 1),)),
             sem((max(units * X, 1),)),
             sem((max(units * X, 1),)),
-            sem((2,)),
-            sem((2,)),
-            sem((2 + 4 * X,)),
-            sem((2 + 4 * X,)),
+            sem((2, PIECES)),
+            sem((2, PIECES)),
+            sem((2 * PIECES + 4 * X,)),
+            sem((2 * PIECES + 4 * X,)),
             sem((4 * max(X - 1, 1),)),
             sem((4 * max(X - 1, 1),)),
         ],

time: 86.3 us -> 71.1 us (0.82)
  the two profiles are of different devices: /device:TPU:16 before, /device:TPU:0 now
where the time goes in v3:
time: 71.1 us; the launch traced here: 70.8 us
  Pallas kernels  65.4 us (92%)
  local copies, waits for them, and re-layouts  4.52 us (6%)
  other arithmetic  0.81 us (1%)
    pallas_call x1, Pallas kernels, shards(): pl.pallas_call(functools.partial(kernel, S, T), out_shape=jax.ShapeDtypeS...  65.4 us
    unnamed x2, local copies, waits for them, and re-layouts  2.51 us

profile of v3, /device:TPU:0, one launch (start us, length us, event | category | flops | bytes accessed | tf_op | source)
XLA Modules:
  0.0 70.8 jit_solution(14854854965709881589)
XLA Ops:
  0.0 0.7 stack.9
  0.7 0.7 stack.10
  1.4 0.1 fusion.2
  1.5 0.6 pad.8.active
  2.1 0.8 %copy.16 = f32[8,15,31]{2,1,0:T(8,128)S(1)} copy(f32[8,15,31]{2,0,1:T(8,128)} %param.28) | data formatting | bytes 29760 | tf_op args[13]
  3.0 0.7 %pad_maximum_fusion.table_rows = f32[8,14,128]{2,1,0:T(8,128)} fusion(f32[8,14,64]{2,1,0:T(8,128)S(1)} %get-tuple-element.6, f32[8,14,64]{2,1,0:T(8,128)S(1)} %get-tuple-element.5), kind=kLoop, calls=%fused_computation | loop fusion | flops 14336 | bytes 114688 | tf_op jit(solution)/shard_map/concatenate | solution.py:593
  3.7 65.4 %shard_map.145 = bf16[64,2048]{1,0:T(8,128)(2,1)} custom-call(bf16[16,256]{1,0:T(8,128)(2,1)} %pad.8.active, f32[1,2048]{1,0:T(1,128)} %bitcast.2, f32[1,2048]{1,0:T(1,128)} %bitcast.3, f32[8,14,128]{2,1,0:T(8,128)} %pad_maximum_fusion.table_rows, bf16[256,2048]{1,0:T(8,128)(2,1)} %latent_hbm.1, bf16[128,2048]{1,0:T(8,128)(2,1)} %context_hbm.1, ...), custom_call_target="tpu_custom_call" | custom-call | tf_op jit(solution)/shard_map/pallas_call | solution.py:601
  69.1 1.7 %copy.18 = bf16[64,2048]{1,0:T(8,128)(2,1)} copy(bf16[64,2048]{1,0:T(8,128)(2,1)} %shard_map.145) | data formatting | bytes 524288
  (1 shorter events, 0.0 us)
